TPU v7x, 128 devices: a whole 4x4x4 slice. The times are simulated.
128 devices in a mesh: sp: 16 (over z, y), dp: 8 (over x, core).
Axes of the slice: x: 4, y: 4, z: 4, core: 2. Of those that a mesh axis runs over, the one named last changes fastest.
Arguments:
- tokens: bfloat16 [8, 4096, 2048], P('dp', 'sp'), may hold values from -6 to 6
- w_query: bfloat16 [2048, 2048], P('dp', 'sp'), may hold values from -0.125 to 0.125
- w_key: bfloat16 [2048, 1024], P('dp', 'sp'), may hold values from -0.125 to 0.125
- w_value: bfloat16 [2048, 1024], P('dp', 'sp'), may hold values from -0.125 to 0.125
- w_out: bfloat16 [2048, 2048], P('dp', 'sp'), may hold values from -0.25 to 0.25
- qk_gain: float32 [2, 128], replicated, may hold values from 0.9 to 24
Outputs:
- mixed_out: bfloat16 [8, 4096, 2048], P('dp', 'sp')
All inputs are finite; a program needn't handle non-finite values.
Results may differ from a plain program's by a relative error of at most 0.006.
The roundings to bfloat16 on the way count: a program that leaves them out, or rounds other values in their place, can miss the bound.
Values may be sent and summed in bfloat16 or wider, within the bound.
A program may use at most 64 MiB of HBM per device.

v0:
```python
import math
import jax
import jax.numpy as jnp
import numpy as np
from jax import lax
from jax.sharding import PartitionSpec as P

HQ = 16
KV = 8
HD = 128
GRID_W = 64
ROPE_BASE = 10000.0
EPS = 1e-06


def in_order(blocks, dim):
    blocks = jnp.moveaxis(blocks, 0, dim)
    shape = blocks.shape
    return blocks.reshape(*shape[:dim], shape[dim] * shape[dim + 1], *shape[dim + 2 :])


def sent_to_all(x, axis):
    copies = jnp.broadcast_to(x, (lax.axis_size(axis), *x.shape))
    return lax.all_to_all(copies, axis, split_axis=0, concat_axis=0, tiled=True)


def collect(x, axis, dim):
    return in_order(sent_to_all(x, axis), dim)


def angles(positions):
    quarter = jnp.arange(0, HD // 2, 2, dtype=jnp.float32)
    inv_freq = ROPE_BASE ** (-quarter / (HD // 2))
    row_pos = (positions // GRID_W).astype(jnp.float32)
    col_pos = (positions % GRID_W).astype(jnp.float32)
    angle_table = jnp.concatenate(
        [row_pos[:, None] * inv_freq, col_pos[:, None] * inv_freq], axis=1
    )
    return (jnp.cos(angle_table), jnp.sin(angle_table))


def prepare(raw_proj, gain_row, cosine, sine_table):
    normed = (
        raw_proj * lax.rsqrt(jnp.mean(raw_proj * raw_proj, axis=-1, keepdims=True) + EPS) * gain_row
    )
    pair_view = normed.reshape(raw_proj.shape[:-1] + (HD // 2, 2))
    first_half = pair_view[..., 0]
    second = pair_view[..., 1]
    cos_b = cosine[:, None, :]
    sin_b = sine_table[:, None, :]
    turned = jnp.stack(
        [first_half * cos_b - second * sin_b, first_half * sin_b + second * cos_b], axis=-1
    )
    return turned.reshape(raw_proj.shape).astype(jnp.bfloat16)


def attend_head(query_rows, key_rows, value_rows):
    seq_len = query_rows.shape[0]
    block_len = math.gcd(seq_len, 512)
    blocks = query_rows.reshape(seq_len // block_len, block_len, HD)

    def one_block(row_block):
        scores = jnp.dot(row_block, key_rows.T, preferred_element_type=jnp.float32) * HD ** (-0.5)
        top_score = jnp.max(scores, axis=1, keepdims=True)
        weights = jnp.exp(scores - top_score)
        row_total = jnp.sum(weights, axis=1, keepdims=True)
        probs_bf = (weights / row_total).astype(jnp.bfloat16)
        return jnp.dot(probs_bf, value_rows, preferred_element_type=jnp.float32).astype(
            jnp.bfloat16
        )

    return lax.map(one_block, blocks).reshape(seq_len, HD)


def project(own_rows, weight):
    col_full = collect(weight, "sp", 1)
    return jnp.dot(
        own_rows,
        lax.all_gather(col_full, "dp", axis=0, tiled=True),
        preferred_element_type=jnp.float32,
    )


def on_device(tokens, w_query, w_key, w_value, w_out, qk_gain):
    own_rows = tokens[0]
    n_seqdev = lax.axis_size("sp")
    tok_local = own_rows.shape[0]
    positions = lax.axis_index("sp") * tok_local + jnp.arange(tok_local, dtype=jnp.int32)
    cosine, sine_table = angles(positions)
    heads_dev = HQ // n_seqdev
    group_size = HQ // KV
    kv_dev = max(1, heads_dev // group_size)
    chosen = (np.arange(n_seqdev) * heads_dev // group_size)[:, None] + np.arange(kv_dev)[None, :]
    chosen = chosen.reshape(-1)
    key_all = prepare(
        project(own_rows, w_key).reshape(tok_local, KV, HD), qk_gain[1], cosine, sine_table
    )
    values = project(own_rows, w_value).astype(jnp.bfloat16).reshape(tok_local, KV, HD)
    key_send = key_all[:, chosen, :].reshape(tok_local, -1)
    value_send = values[:, chosen, :].reshape(tok_local, -1)
    raw_proj = project(own_rows, w_query).reshape(tok_local, HQ, HD)
    query_heads = lax.all_to_all(
        prepare(raw_proj, qk_gain[0], cosine, sine_table).reshape(tok_local, HQ * HD),
        "sp",
        split_axis=1,
        concat_axis=0,
        tiled=True,
    )
    key_heads = lax.all_to_all(key_send, "sp", split_axis=1, concat_axis=0, tiled=True)
    value_heads = lax.all_to_all(value_send, "sp", split_axis=1, concat_axis=0, tiled=True)
    outputs = attend_head(query_heads, key_heads[:, 0:HD], value_heads[:, 0:HD])
    token_rows = lax.all_to_all(outputs, "sp", split_axis=0, concat_axis=1, tiled=True)
    return project(token_rows, w_out).astype(jnp.bfloat16)[None]


def solution(mesh):
    in_specs = (
        P("dp", "sp", None),
        P("dp", "sp"),
        P("dp", "sp"),
        P("dp", "sp"),
        P("dp", "sp"),
        P(),
    )
    out_specs = P("dp", "sp", None)
    return jax.shard_map(
        on_device, mesh=mesh, in_specs=in_specs, out_specs=out_specs, check_vma=False
    )
```

profile of v0, /device:TPU:0, one launch (start us, length us, event | category | flops | bytes accessed | tf_op | source)
XLA Modules:
  0.0 289.2 jit_solution(16202396729736009710)
XLA Ops:
  7.5 19.6 %all_to_all.84 = bf16[16,256,64]{1,2,0:T(8,128)(2,1)} all-to-all(bf16[16,256,64]{1,2,0:T(8,128)(2,1)S(1)} %broadcast_in_dim.42), channel_id=1, replica_groups=mesh['sp'=16,'dp'=8] {'sp'}, dimensions={0} | all-to-all | bytes 1048576 | tf_op jit(solution)/shard_map/all_to_all | solution.py:24
  28.0 13.8 %all_to_all.85 = bf16[16,256,64]{1,2,0:T(8,128)(2,1)} all-to-all(bf16[16,256,64]{1,2,0:T(8,128)(2,1)S(1)} %broadcast_in_dim.44), channel_id=1, replica_groups=mesh['sp'=16,'dp'=8] {'sp'}, dimensions={0} | all-to-all | bytes 1048576 | tf_op jit(solution)/shard_map/all_to_all | solution.py:24
  42.9 18.8 %all_to_all.86 = bf16[16,256,128]{1,2,0:T(8,128)(2,1)} all-to-all(bf16[16,256,128]{1,2,0:T(8,128)(2,1)S(1)} %broadcast_in_dim.23), channel_id=1, replica_groups=mesh['sp'=16,'dp'=8] {'sp'}, dimensions={0} | all-to-all | bytes 2097152 | tf_op jit(solution)/shard_map/all_to_all | solution.py:24
  62.9 3.7 %all-to-all-start.7 = ((bf16[16,256,128]{1,2,0:T(8,128)(2,1)}), bf16[16,256,128]{1,2,0:T(8,128)(2,1)S(1)}, u32[]{:S(2)}, u32[]{:S(2)}) async-start(bf16[16,256,128]{1,2,0:T(8,128)(2,1)} %broadcast_in_dim.46), calls=%async_computation.7 | async-start | bytes 2097152 | tf_op jit(solution)/shard_map/all_to_all | solution.py:24
  67.0 3.5 %multiply_reduce_fusion.2 = (f32[256,8]{0,1:T(8,128)S(1)}, f32[256,8,128]{0,2,1:T(8,128)S(1)}) fusion(bf16[8,128,2048]{2,1,0:T(8,128)(2,1)} %bitcast.98, bf16[1,256,2048]{2,1,0:T(8,128)(2,1)S(1)} %copy-done), kind=kOutput, calls=%fused_computation.28 | convolution fusion | flops 1074264064 | bytes 6299648 | tf_op jit(solution)/shard_map/dot_general | solution.py:77
  73.7 7.9 %all-to-all-done.7 = bf16[16,256,128]{1,2,0:T(8,128)(2,1)S(1)} async-done(((bf16[16,256,128]{1,2,0:T(8,128)(2,1)}), bf16[16,256,128]{1,2,0:T(8,128)(2,1)S(1)}, u32[]{:S(2)}, u32[]{:S(2)}) %all-to-all-start.7) | async-done | bytes 1048608 | tf_op jit(solution)/shard_map/all_to_all | solution.py:24
  82.6 3.7 %all-to-all-start.3 = ((bf16[256,16,128]{2,0,1:T(8,128)(2,1)}), bf16[256,16,128]{2,0,1:T(8,128)(2,1)S(1)}, u32[]{:S(2)}, u32[]{:S(2)}) async-start(bf16[256,16,128]{2,0,1:T(8,128)(2,1)} %bitcast.17), calls=%async_computation.3 | async-start | bytes 2097152 | tf_op jit(solution)/shard_map/all_to_all | solution.py:109
  86.3 12.1 %all-gather.9.cloned.1.call-done = bf16[2048,1024]{0,1:T(8,128)(2,1)} async-done(((bf16[256,1024]{0,1:T(8,128)(2,1)}), bf16[2048,1024]{0,1:T(8,128)(2,1)}) %all-gather.9.cloned.1.call-update) | async-done | bytes 4194320 | tf_op jit(solution)/shard_map/all_gather | solution.py:79
  98.4 3.5 %fusion.11 = bf16[32,8,8,128]{3,2,1,0:T(8,128)(2,1)S(1)} fusion(bf16[2048,1024]{0,1:T(8,128)(2,1)} %all-gather.9.cloned.1.call-done, bf16[1,256,2048]{2,1,0:T(8,128)(2,1)S(1)} %copy-done), kind=kOutput, calls=%fused_computation.20 | convolution fusion | flops 1074003968 | bytes 5767168 | tf_op jit(solution)/shard_map/dot_general | solution.py:77
  103.6 50.8 %all-gather.5.cloned.1.call-done = bf16[2048,2048]{0,1:T(8,128)(2,1)} async-done(((bf16[256,2048]{0,1:T(8,128)(2,1)}), bf16[2048,2048]{0,1:T(8,128)(2,1)}) %all-gather.5.cloned.1.call-update) | async-done | bytes 8388624 | tf_op jit(solution)/shard_map/all_gather | solution.py:79
  154.4 7.2 %multiply_reduce_fusion.1 = (f32[256,16]{0,1:T(8,128)S(1)}, f32[256,16,128]{0,2,1:T(8,128)}) fusion(bf16[16,128,2048]{2,1,0:T(8,128)(2,1)} %bitcast.97, bf16[1,256,2048]{2,1,0:T(8,128)(2,1)S(1)} %copy-done), kind=kOutput, calls=%fused_computation.18 | convolution fusion | flops 2148528128 | bytes 11550720 | tf_op jit(solution)/shard_map/dot_general | solution.py:77
  161.6 7.1 %all-to-all-start.5 = ((bf16[256,16,128]{2,0,1:T(8,128)(2,1)}), bf16[256,16,128]{2,0,1:T(8,128)(2,1)}, u32[]{:S(2)}, u32[]{:S(2)}) async-start(bf16[256,16,128]{2,0,1:T(8,128)(2,1)} %bitcast.22), calls=%async_computation.5 | async-start | bytes 2097152 | tf_op jit(solution)/shard_map/all_to_all | solution.py:110
  168.7 3.3 %multiply_multiply_fusion = f32[256,16,128]{0,2,1:T(8,128)} fusion(f32[256,16,128]{0,2,1:T(8,128)} %get-tuple-element.56, f32[128]{0:T(128)S(1)} %get-tuple-element.52, f32[256,16]{0,1:T(8,128)S(1)} %add_rsqrt_fusion), kind=kLoop, calls=%fused_computation.17 | loop fusion | flops 1048576 | bytes 4211200 | tf_op jit(solution)/shard_map/mul | solution.py:44
  172.0 3.4 %reshape.170 = f32[256,16,64,2]{0,3,2,1:T(2,128)} reshape(f32[256,16,128]{0,2,1:T(8,128)} %multiply_multiply_fusion) | data formatting | bytes 4194304 | tf_op jit(solution)/shard_map/reshape | solution.py:46
  175.4 4.3 %subtract_convert_fusion = (bf16[256,16,64,1]{0,3,2,1:T(2,128)(2,1)S(1)}, bf16[256,16,64,1]{0,3,2,1:T(2,128)(2,1)S(1)}) fusion(f32[256,16,64,2]{0,3,2,1:T(2,128)} %reshape.170, f32[256,64]{0,1:T(8,128)S(1)} %get-tuple-element.50, f32[256,64]{0,1:T(8,128)S(1)} %get-tuple-element.49), kind=kLoop, calls=%fused_computation.30 | loop fusion | flops 2097152 | bytes 3276800 | tf_op jit(solution)/shard_map/convert.2
  186.6 4.5 %all-to-all-start.1 = ((bf16[256,16,128]{2,0,1:T(8,128)(2,1)}), bf16[256,16,128]{2,0,1:T(8,128)(2,1)S(1)}, u32[]{:S(2)}, u32[]{:S(2)}) async-start(bf16[256,16,128]{2,0,1:T(8,128)(2,1)} %copy.20), calls=%async_computation.1 | async-start | bytes 2097152 | tf_op jit(solution)/shard_map/all_to_all | solution.py:102
  191.7 16.9 %all-to-all-done.1 = bf16[256,16,128]{2,0,1:T(8,128)(2,1)S(1)} async-done(((bf16[256,16,128]{2,0,1:T(8,128)(2,1)}), bf16[256,16,128]{2,0,1:T(8,128)(2,1)S(1)}, u32[]{:S(2)}, u32[]{:S(2)}) %all-to-all-start.1) | async-done | bytes 1048608 | tf_op jit(solution)/shard_map/all_to_all | solution.py:102
  208.6 47.3 %while.10 = (s32[]{:T(128)}, bf16[8,512,128]{2,1,0:T(8,128)(2,1)S(1)}, bf16[8,512,128]{2,1,0:T(8,128)(2,1)S(1)}, bf16[4096,128]{1,0:T(8,128)(2,1)S(1)}, bf16[4096,128]{1,0:T(8,128)(2,1)}, /*index=5*/s32[]{:T(128)}) while((s32[]{:T(128)}, bf16[8,512,128]{2,1,0:T(8,128)(2,1)S(1)}, bf16[8,512,128]{2,1,0:T(8,128)(2,1)S(1)}, ...), condition=%wide.region_5.6_spmd, body=%wide.region_2.5_spmd.sunk | while | flops 1092680704 | bytes 27535436 | solution.py:72
  211.5 3.1 %fusion.36 = bf16[8,512,128]{2,1,0:T(8,128)(2,1)S(1)} fusion(bf16[8,512,128]{2,1,0:T(8,128)(2,1)S(1)} %get-tuple-element.103, s32[]{:T(128)} %get-tuple-element.102, bf16[4096,128]{1,0:T(8,128)(2,1)} %get-tuple-element.112, f32[512,4096]{1,0:T(8,128)S(1)} %get-tuple-element.94, f32[512]{0:T(512)S(1)} %fusion.35, f32[512]{0:T(512)S(1)} %get-tuple-element.95), kind=kOutput, calls=%fused_computation.9.clone.1 | convolution fusion | flops 545325056 | bytes 9572356 | tf_op jit(solution)/shard_map/while/body/eval_jaxpr/dot_general | solution.py:68
  217.4 3.1 %fusion.36 = bf16[8,512,128]{2,1,0:T(8,128)(2,1)S(1)} fusion(bf16[8,512,128]{2,1,0:T(8,128)(2,1)S(1)} %get-tuple-element.103, s32[]{:T(128)} %get-tuple-element.102, bf16[4096,128]{1,0:T(8,128)(2,1)} %get-tuple-element.112, f32[512,4096]{1,0:T(8,128)S(1)} %get-tuple-element.94, f32[512]{0:T(512)S(1)} %fusion.35, f32[512]{0:T(512)S(1)} %get-tuple-element.95), kind=kOutput, calls=%fused_computation.9.clone.1 | convolution fusion | flops 545325056 | bytes 9572356 | tf_op jit(solution)/shard_map/while/body/eval_jaxpr/dot_general | solution.py:68
  223.3 3.1 %fusion.36 = bf16[8,512,128]{2,1,0:T(8,128)(2,1)S(1)} fusion(bf16[8,512,128]{2,1,0:T(8,128)(2,1)S(1)} %get-tuple-element.103, s32[]{:T(128)} %get-tuple-element.102, bf16[4096,128]{1,0:T(8,128)(2,1)} %get-tuple-element.112, f32[512,4096]{1,0:T(8,128)S(1)} %get-tuple-element.94, f32[512]{0:T(512)S(1)} %fusion.35, f32[512]{0:T(512)S(1)} %get-tuple-element.95), kind=kOutput, calls=%fused_computation.9.clone.1 | convolution fusion | flops 545325056 | bytes 9572356 | tf_op jit(solution)/shard_map/while/body/eval_jaxpr/dot_general | solution.py:68
  235.1 3.1 %fusion.36 = bf16[8,512,128]{2,1,0:T(8,128)(2,1)S(1)} fusion(bf16[8,512,128]{2,1,0:T(8,128)(2,1)S(1)} %get-tuple-element.103, s32[]{:T(128)} %get-tuple-element.102, bf16[4096,128]{1,0:T(8,128)(2,1)} %get-tuple-element.112, f32[512,4096]{1,0:T(8,128)S(1)} %get-tuple-element.94, f32[512]{0:T(512)S(1)} %fusion.35, f32[512]{0:T(512)S(1)} %get-tuple-element.95), kind=kOutput, calls=%fused_computation.9.clone.1 | convolution fusion | flops 545325056 | bytes 9572356 | tf_op jit(solution)/shard_map/while/body/eval_jaxpr/dot_general | solution.py:68
  256.0 19.4 %all_to_all.87 = bf16[16,256,128]{2,1,0:T(8,128)(2,1)S(1)} all-to-all(bf16[16,256,128]{2,1,0:T(8,128)(2,1)S(1)} %bitcast.95), channel_id=1, replica_groups=mesh['sp'=16,'dp'=8] {'sp'}, dimensions={0} | all-to-all | bytes 2097152 | tf_op jit(solution)/shard_map/all_to_all | solution.py:112
  276.0 6.7 %fusion.10 = bf16[1,256,2048]{2,1,0:T(8,128)(2,1)} fusion(bf16[256,2048]{0,1:T(8,128)(2,1)S(1)} %bitcast.96, bf16[2048,2048]{0,1:T(8,128)(2,1)} %all-gather.11.cloned.1.call-done), kind=kOutput, calls=%fused_computation.16 | convolution fusion | flops 2148007936 | bytes 10485760 | tf_op jit(solution)/shard_map/dot_general | solution.py:77
  (71 shorter events, 53.3 us)
Async XLA Ops:
  6.5 60.5 %copy-start = (bf16[1,256,2048]{2,1,0:T(8,128)(2,1)S(1)}, bf16[1,256,2048]{2,1,0:T(8,128)(2,1)}, u32[]{:S(2)}) copy-start(bf16[1,256,2048]{2,1,0:T(8,128)(2,1)} %param.11) | copy-start | bytes 3145732
  6.5 60.1 %copy-start.5 = (s32[16]{0:T(128)S(1)}, s32[16]{0:T(128)}, u32[]{:S(2)}) copy-start(s32[16]{0:T(128)} %constant.81) | copy-start | bytes 196
  6.5 55.2 %copy-start.3 = (bf16[256,128]{1,0:T(8,128)(2,1)S(1)}, bf16[256,128]{1,0:T(8,128)(2,1)}, u32[]{:S(2)}) copy-start(bf16[256,128]{1,0:T(8,128)(2,1)} %param.15) | copy-start | bytes 196612
  6.5 60.4 %copy-start.4 = (f32[2,128]{1,0:T(2,128)S(1)}, f32[2,128]{1,0:T(2,128)}, u32[]{:S(2)}) copy-start(f32[2,128]{1,0:T(2,128)} %param.16) | copy-start | bytes 3076
  6.5 60.5 %all-gather.7.cloned.1.call-start = ((), (), s32[]{:S(2)}) async-start(), calls=%async_computation.9 | async-start | bytes 4718592 | tf_op jit(solution)/shard_map/all_gather | solution.py:79
  27.1 71.3 %all-gather.9.cloned.1.call-start = ((), (), s32[]{:S(2)}) async-start(), calls=%async_computation.10 | async-start | bytes 4718592 | tf_op jit(solution)/shard_map/all_gather | solution.py:79
  41.8 112.6 %all-gather.5.cloned.1.call-start = ((), (), s32[]{:S(2)}) async-start(), calls=%async_computation.8 | async-start | bytes 9437184 | tf_op jit(solution)/shard_map/all_gather | solution.py:79
  62.9 18.6 %all-to-all-start.7 = ((bf16[16,256,128]{1,2,0:T(8,128)(2,1)}), bf16[16,256,128]{1,2,0:T(8,128)(2,1)S(1)}, u32[]{:S(2)}, u32[]{:S(2)}) async-start(bf16[16,256,128]{1,2,0:T(8,128)(2,1)} %broadcast_in_dim.46), calls=%async_computation.7 | async-start | bytes 2097152 | tf_op jit(solution)/shard_map/all_to_all | solution.py:24
  81.5 1.0 copy-start.2
  82.6 79.0 %all-to-all-start.3 = ((bf16[256,16,128]{2,0,1:T(8,128)(2,1)}), bf16[256,16,128]{2,0,1:T(8,128)(2,1)S(1)}, u32[]{:S(2)}, u32[]{:S(2)}) async-start(bf16[256,16,128]{2,0,1:T(8,128)(2,1)} %bitcast.17), calls=%async_computation.3 | async-start | bytes 2097152 | tf_op jit(solution)/shard_map/all_to_all | solution.py:109
  161.6 25.0 %all-to-all-start.5 = ((bf16[256,16,128]{2,0,1:T(8,128)(2,1)}), bf16[256,16,128]{2,0,1:T(8,128)(2,1)}, u32[]{:S(2)}, u32[]{:S(2)}) async-start(bf16[256,16,128]{2,0,1:T(8,128)(2,1)} %bitcast.22), calls=%async_computation.5 | async-start | bytes 2097152 | tf_op jit(solution)/shard_map/all_to_all | solution.py:110
  186.6 22.0 %all-to-all-start.1 = ((bf16[256,16,128]{2,0,1:T(8,128)(2,1)}), bf16[256,16,128]{2,0,1:T(8,128)(2,1)S(1)}, u32[]{:S(2)}, u32[]{:S(2)}) async-start(bf16[256,16,128]{2,0,1:T(8,128)(2,1)} %copy.20), calls=%async_computation.1 | async-start | bytes 2097152 | tf_op jit(solution)/shard_map/all_to_all | solution.py:102
  191.1 84.8 %all-gather.11.cloned.1.call-start = ((), (), s32[]{:S(2)}) async-start(), calls=%async_computation.11 | async-start | bytes 9437184 | tf_op jit(solution)/shard_map/all_gather | solution.py:79
  275.4 7.3 %copy-start.1 = (bf16[1,256,2048]{2,1,0:T(8,128)(2,1)S(1)}, bf16[1,256,2048]{2,1,0:T(8,128)(2,1)}, u32[]{:S(2)}) copy-start(bf16[1,256,2048]{2,1,0:T(8,128)(2,1)} %param.11) | copy-start | bytes 3145732
Sparse Core Ops, SparseCore 0:
  27.2 32.9 all-gather.6
  61.9 36.4 all-gather.8
  100.0 54.3 all-gather.4
  193.3 54.5 all-gather.10
where the time goes:
time: 290 us; the launch traced here: 289 us
  waiting for transfers between devices  91 us (31%)
  blocking collectives  71.7 us (25%)
  matrix products  56 us (19%)
  other arithmetic  22.9 us (8%)
  starting transfers between devices  19 us (7%)
  local copies, waits for them, and re-layouts  15.2 us (5%)
  between operations  13.4 us (5%)
    all_gather x4, waiting for transfers between devices, project(): lax.all_gather(col_full, 'dp', axis=0, tiled=True)  62.9 us
    all_to_all x3, blocking collectives, sent_to_all(): return lax.all_to_all(copies, axis, split_axis=0, concat_axis=0, tiled=True)  52.2 us
    dot_general x8, matrix products, one_block(): jnp.dot(probs_bf, value_rows, preferred_element_type=jnp.float32)  24.5 us
    dot_general x4, matrix products, project(): jnp.dot(own_rows, lax.all_gather(col_full, 'dp', axis=0, tiled=True), pre...  20.9 us
    all_to_all x1, blocking collectives, on_device(): lax.all_to_all(outputs, 'sp', split_axis=0, concat_axis=1, tiled=True)  19.4 us
    all_to_all x1, waiting for transfers between devices, on_device(): lax.all_to_all(prepare(raw_proj, qk_gain[0], cosine, sine_table).reshape(...  16.9 us
    reduce_sum x8, other arithmetic, one_block(): row_total = jnp.sum(weights, axis=1, keepdims=True)  12.1 us
    dot_general x8, matrix products, one_block(): jnp.dot(row_block, key_rows.T, preferred_element_type=jnp.float32)  10.7 us
  transfers between devices with their start and end apart: 8, of which 5 were waited for; matrix products, arithmetic and copies ran while one was open for 30% of the time, Pallas kernels for 0%

commit v1 on v0

--- a/solution.py
+++ b/solution.py
@@ -74,10 +74,36 @@
 
 def project(own_rows, weight):
     col_full = collect(weight, "sp", 1)
+
+    def treat_panels_on(xin, mesh_dim):
+        known, a_next, mat_out = (lax.axis_size(mesh_dim), lax.axis_index(mesh_dim), xin.shape[0])
+        reached = lax.dynamic_update_slice_in_dim(
+            jnp.zeros([k0 * known if h == 0 else k0 for h, k0 in enumerate(xin.shape)], xin.dtype),
+            xin,
+            a_next * mat_out,
+            axis=0,
+        )
+        r2 = spare = xin
+        for q in range(1, known // 2 + 1):
+            r2 = lax.ppermute(
+                r2, axis_name=mesh_dim, perm=list(map(lambda h: (h, (h + 1) % known), range(known)))
+            )
+            reached = lax.dynamic_update_slice_in_dim(
+                reached, r2, (a_next - q) % known * mat_out, axis=0
+            )
+            if 2 * q < known:
+                spare = lax.ppermute(
+                    spare,
+                    axis_name=mesh_dim,
+                    perm=list(map(lambda h: (h, (h - 1) % known), range(known))),
+                )
+                reached = lax.dynamic_update_slice_in_dim(
+                    reached, spare, (a_next + q) % known * mat_out, axis=0
+                )
+        return reached
+
     return jnp.dot(
-        own_rows,
-        lax.all_gather(col_full, "dp", axis=0, tiled=True),
-        preferred_element_type=jnp.float32,
+        own_rows, treat_panels_on(col_full, mesh_dim="dp"), preferred_element_type=jnp.float32
     )
 
 

time: 290 us -> 331 us (1.14)
  the two profiles are of different devices: /device:TPU:0 before, /device:TPU:7 now
where the time goes in v1:
time: 331 us; the launch traced here: 329 us
  local copies, waits for them, and re-layouts  96.2 us (29%)
  starting transfers between devices  69.4 us (21%)
  waiting for transfers between devices  56.7 us (17%)
  matrix products  53.8 us (16%)
  blocking collectives  31.3 us (9%)
  other arithmetic  21.3 us (6%)
    ppermute x16, starting transfers between devices, treat_panels_on(): lax.ppermute(r2, axis_name=mesh_dim, perm=list(map(lambda h: (h, (h + 1)...  33.9 us
    all_to_all x2, blocking collectives, sent_to_all(): return lax.all_to_all(copies, axis, split_axis=0, concat_axis=0, tiled=True)  31.3 us
    dynamic_update_slice x15, local copies, waits for them, and re-layouts, treat_panels_on(): lax.dynamic_update_slice_in_dim(reached, r2, (a_next - q) % known * mat_o...  28.5 us
    ppermute x16, waiting for transfers between devices, treat_panels_on(): lax.ppermute(r2, axis_name=mesh_dim, perm=list(map(lambda h: (h, (h + 1)...  23.5 us
    dot_general x4, matrix products, project(): jnp.dot(own_rows, treat_panels_on(col_full, mesh_dim='dp'), preferred_ele...  22.7 us
    dynamic_update_slice x12, local copies, waits for them, and re-layouts, treat_panels_on(): lax.dynamic_update_slice_in_dim(reached, spare, (a_next + q) % known * ma...  22.4 us
    dot_general x8, matrix products, one_block(): jnp.dot(probs_bf, value_rows, preferred_element_type=jnp.float32)  20.4 us
    all_to_all x2, waiting for transfers between devices, sent_to_all(): return lax.all_to_all(copies, axis, split_axis=0, concat_axis=0, tiled=True)  14.8 us
  transfers between devices with their start and end apart: 34, of which 8 were waited for; matrix products, arithmetic and copies ran while one was open for 48% of the time, Pallas kernels for 0%

profile of v1, /device:TPU:7, one launch (start us, length us, event | category | flops | bytes accessed | tf_op | source)
XLA Modules:
  0.0 329.4 jit_solution(11427762107101018924)
XLA Ops:
  0.9 18.1 %all_to_all.84 = bf16[16,256,64]{1,2,0:T(8,128)(2,1)} all-to-all(bf16[16,256,64]{1,2,0:T(8,128)(2,1)S(1)} %broadcast_in_dim.44), channel_id=1, replica_groups=mesh['sp'=16,'dp'=8] {'sp'}, dimensions={0} | all-to-all | bytes 1048576 | tf_op jit(solution)/shard_map/all_to_all | solution.py:24
  19.8 13.2 %all_to_all.85 = bf16[16,256,64]{1,2,0:T(8,128)(2,1)} all-to-all(bf16[16,256,64]{1,2,0:T(8,128)(2,1)S(1)} %broadcast_in_dim.42), channel_id=1, replica_groups=mesh['sp'=16,'dp'=8] {'sp'}, dimensions={0} | all-to-all | bytes 1048576 | tf_op jit(solution)/shard_map/all_to_all | solution.py:24
  35.1 3.7 %all-to-all-start = ((bf16[16,256,128]{2,1,0:T(8,128)(2,1)}), bf16[16,256,128]{2,1,0:T(8,128)(2,1)S(1)}, u32[]{:S(2)}, u32[]{:S(2)}) async-start(bf16[16,256,128]{2,1,0:T(8,128)(2,1)} %broadcast_in_dim.23), calls=%async_computation | async-start | bytes 2097152 | tf_op jit(solution)/shard_map/all_to_all | solution.py:24
  38.7 14.8 %all-to-all-done = bf16[16,256,128]{2,1,0:T(8,128)(2,1)S(1)} async-done(((bf16[16,256,128]{2,1,0:T(8,128)(2,1)}), bf16[16,256,128]{2,1,0:T(8,128)(2,1)S(1)}, u32[]{:S(2)}, u32[]{:S(2)}) %all-to-all-start) | async-done | bytes 1048608 | tf_op jit(solution)/shard_map/all_to_all | solution.py:24
  55.5 4.3 %all-to-all-start.7 = ((bf16[16,256,128]{2,1,0:T(8,128)(2,1)}), bf16[16,256,128]{2,1,0:T(8,128)(2,1)}, u32[]{:S(2)}, u32[]{:S(2)}) async-start(bf16[16,256,128]{2,1,0:T(8,128)(2,1)} %broadcast_in_dim.46), calls=%async_computation.7 | async-start | bytes 2097152 | tf_op jit(solution)/shard_map/all_to_all | solution.py:24
  59.9 3.8 %collective-permute-start.14 = (bf16[256,1024]{0,1:T(8,128)(2,1)}, bf16[256,1024]{0,1:T(8,128)(2,1)}, u32[]{:S(2)}, u32[]{:S(2)}) collective-permute-start(bf16[256,1024]{0,1:T(8,128)(2,1)} %bitcast.20), channel_id=1, source_target_pairs={{0,1},{1,2},{2,3},{3,4},{4,5},{5,6},{6,7},{7,0},{8,9},{9,10},{10,1... | collective-permute-start | bytes 1572872 | tf_op jit(solution)/shard_map/ppermute | solution.py:88
  70.1 3.7 %collective-permute-start.16 = (bf16[256,1024]{0,1:T(8,128)(2,1)}, bf16[256,1024]{0,1:T(8,128)(2,1)}, u32[]{:S(2)}, u32[]{:S(2)}) collective-permute-start(bf16[256,1024]{0,1:T(8,128)(2,1)} %collective-permute-done.14), channel_id=1, source_target_pairs={{0,1},{1,2},{2,3},{3,4},{4,5},{5,6},{6,7},{7,0},{8,9},{9,10},{10,1... | collective-permute-start | bytes 1572872 | tf_op jit(solution)/shard_map/ppermute | solution.py:88
  88.6 4.3 %broadcast.154.clone = bf16[2048,2048]{0,1:T(8,128)(2,1)} broadcast(bf16[]{:T(256)} %constant.150.clone.1), dimensions={} | broadcast | bytes 8388610 | tf_op jit(solution)/shard_map/broadcast.8
  131.0 13.0 %collective-permute-done.20 = bf16[256,1024]{0,1:T(8,128)(2,1)S(1)} collective-permute-done((bf16[256,1024]{0,1:T(8,128)(2,1)S(1)}, bf16[256,1024]{0,1:T(8,128)(2,1)S(1)}, u32[]{:S(2)}, u32[]{:S(2)}) %collective-permute-start.20) | collective-permute-done | bytes 524320 | tf_op jit(solution)/shard_map/ppermute | solution.py:88
  144.1 5.6 %collective-permute-done.13 = bf16[256,1024]{0,1:T(8,128)(2,1)S(1)} collective-permute-done((bf16[256,1024]{0,1:T(8,128)(2,1)S(1)}, bf16[256,1024]{0,1:T(8,128)(2,1)S(1)}, u32[]{:S(2)}, u32[]{:S(2)}) %collective-permute-start.13) | collective-permute-done | bytes 524320 | tf_op jit(solution)/shard_map/ppermute | solution.py:88
  150.8 3.7 %collective-permute-start.4 = (bf16[256,2048]{0,1:T(8,128)(2,1)}, bf16[256,2048]{0,1:T(8,128)(2,1)}, u32[]{:S(2)}, u32[]{:S(2)}) collective-permute-start(bf16[256,2048]{0,1:T(8,128)(2,1)} %collective-permute-done.2), channel_id=1, source_target_pairs={{0,1},{1,2},{2,3},{3,4},{4,5},{5,6},{6,7},{7,0},{8,9},{9,10},{10,1... | collective-permute-start | bytes 3145736 | tf_op jit(solution)/shard_map/ppermute | solution.py:88
  154.5 4.5 %bitcast_reduce_fusion.1 = (f32[256,8]{0,1:T(8,128)S(1)}, f32[256,1024]{0,1:T(8,128)}) fusion(bf16[2048,1024]{0,1:T(8,128)(2,1)} %get-tuple-element.62, bf16[1,256,2048]{2,1,0:T(8,128)(2,1)S(1)} %copy-done), kind=kOutput, calls=%fused_computation.23 | convolution fusion | flops 1074264064 | bytes 6299648 | tf_op jit(solution)/shard_map/dot_general | solution.py:105
  163.8 6.8 %all-to-all-start.3 = ((bf16[256,16,128]{2,0,1:T(8,128)(2,1)}), bf16[256,16,128]{2,0,1:T(8,128)(2,1)S(1)}, u32[]{:S(2)}, u32[]{:S(2)}) async-start(bf16[256,16,128]{2,0,1:T(8,128)(2,1)} %bitcast.88), calls=%async_computation.3 | async-start | bytes 2097152 | tf_op jit(solution)/shard_map/all_to_all | solution.py:135
  172.2 3.7 %collective-permute-start.6 = (bf16[256,2048]{0,1:T(8,128)(2,1)}, bf16[256,2048]{0,1:T(8,128)(2,1)}, u32[]{:S(2)}, u32[]{:S(2)}) collective-permute-start(bf16[256,2048]{0,1:T(8,128)(2,1)} %collective-permute-done.4), channel_id=1, source_target_pairs={{0,1},{1,2},{2,3},{3,4},{4,5},{5,6},{6,7},{7,0},{8,9},{9,10},{10,1... | collective-permute-start | bytes 3145736 | tf_op jit(solution)/shard_map/ppermute | solution.py:88
  175.9 4.3 %convolution_convert_fusion.1 = bf16[1024,256]{1,0:T(8,128)(2,1)} fusion(bf16[2048,1024]{0,1:T(8,128)(2,1)} %get-tuple-element.61, bf16[1,256,2048]{2,1,0:T(8,128)(2,1)S(1)} %copy-done), kind=kOutput, calls=%fused_computation.21 | convolution fusion | flops 1074003968 | bytes 5767168 | tf_op jit(solution)/shard_map/dot_general | solution.py:105
  194.7 7.2 %bitcast_reduce_fusion = (f32[256,16]{0,1:T(8,128)S(1)}, f32[256,2048]{0,1:T(8,128)}) fusion(bf16[2048,2048]{0,1:T(8,128)(2,1)} %constant_dynamic-update-slice_fusion.24, bf16[1,256,2048]{2,1,0:T(8,128)(2,1)S(1)} %copy-done), kind=kOutput, calls=%fused_computation.18 | convolution fusion | flops 2148528128 | bytes 11550720 | tf_op jit(solution)/shard_map/dot_general | solution.py:105
  205.3 6.9 %all-to-all-start.5 = ((bf16[256,16,128]{0,2,1:T(8,128)(2,1)}), bf16[256,16,128]{0,2,1:T(8,128)(2,1)}, u32[]{:S(2)}, u32[]{:S(2)}) async-start(bf16[256,16,128]{0,2,1:T(8,128)(2,1)} %bitcast.87), calls=%async_computation.5 | async-start | bytes 2097152 | tf_op jit(solution)/shard_map/all_to_all | solution.py:136
  223.7 4.7 %all-to-all-done.5 = bf16[256,16,128]{0,2,1:T(8,128)(2,1)} async-done(((bf16[256,16,128]{0,2,1:T(8,128)(2,1)}), bf16[256,16,128]{0,2,1:T(8,128)(2,1)}, u32[]{:S(2)}, u32[]{:S(2)}) %all-to-all-start.5) | async-done | bytes 1048608 | tf_op jit(solution)/shard_map/all_to_all | solution.py:136
  228.5 4.5 %all-to-all-start.1 = ((bf16[256,16,128]{2,0,1:T(8,128)(2,1)}), bf16[256,16,128]{2,0,1:T(8,128)(2,1)S(1)}, u32[]{:S(2)}, u32[]{:S(2)}) async-start(bf16[256,16,128]{2,0,1:T(8,128)(2,1)} %copy.28), calls=%async_computation.1 | async-start | bytes 2097152 | tf_op jit(solution)/shard_map/all_to_all | solution.py:128
  233.0 4.3 %broadcast.154.clone.1 = bf16[2048,2048]{0,1:T(8,128)(2,1)} broadcast(bf16[]{:T(256)} %constant.150.clone.1), dimensions={} | broadcast | bytes 8388610 | tf_op jit(solution)/shard_map/broadcast.8
  250.9 43.5 %while.10 = (s32[]{:T(128)}, bf16[8,512,128]{2,1,0:T(8,128)(2,1)S(1)}, bf16[8,512,128]{2,1,0:T(8,128)(2,1)S(1)}, bf16[4096,128]{1,0:T(8,128)(2,1)S(1)}, bf16[4096,128]{1,0:T(8,128)(2,1)}, /*index=5*/s32[]{:T(128)}) while((s32[]{:T(128)}, bf16[8,512,128]{2,1,0:T(8,128)(2,1)S(1)}, bf16[8,512,128]{2,1,0:T(8,128)(2,1)S(1)}, ...), condition=%wide.region_5.6_spmd, body=%wide.region_2.5_spmd.sunk | while | flops 1092680704 | bytes 31729776 | solution.py:72
  295.4 6.6 %all-to-all-start.6 = ((bf16[16,256,128]{2,1,0:T(8,128)(2,1)}), bf16[16,256,128]{2,1,0:T(8,128)(2,1)S(1)}, u32[]{:S(2)}, u32[]{:S(2)}) async-start(bf16[16,256,128]{2,1,0:T(8,128)(2,1)} %bitcast.93), calls=%async_computation.6 | async-start | bytes 2097152 | tf_op jit(solution)/shard_map/all_to_all | solution.py:138
  311.4 10.7 %all-to-all-done.6 = bf16[16,256,128]{2,1,0:T(8,128)(2,1)S(1)} async-done(((bf16[16,256,128]{2,1,0:T(8,128)(2,1)}), bf16[16,256,128]{2,1,0:T(8,128)(2,1)S(1)}, u32[]{:S(2)}, u32[]{:S(2)}) %all-to-all-start.6) | async-done | bytes 1048608 | tf_op jit(solution)/shard_map/all_to_all | solution.py:138
  322.6 6.7 %fusion.10 = bf16[1,256,2048]{2,1,0:T(8,128)(2,1)} fusion(bf16[256,2048]{0,1:T(8,128)(2,1)S(1)} %bitcast.95, bf16[2048,2048]{0,1:T(8,128)(2,1)} %constant_dynamic-update-slice_fusion), kind=kOutput, calls=%fused_computation.17 | convolution fusion | flops 2148007936 | bytes 10485760 | tf_op jit(solution)/shard_map/dot_general | solution.py:105
  (170 shorter events, 169.4 us)
Async XLA Ops:
  35.1 18.4 %all-to-all-start = ((bf16[16,256,128]{2,1,0:T(8,128)(2,1)}), bf16[16,256,128]{2,1,0:T(8,128)(2,1)S(1)}, u32[]{:S(2)}, u32[]{:S(2)}) async-start(bf16[16,256,128]{2,1,0:T(8,128)(2,1)} %broadcast_in_dim.23), calls=%async_computation | async-start | bytes 2097152 | tf_op jit(solution)/shard_map/all_to_all | solution.py:24
  55.5 28.7 %all-to-all-start.7 = ((bf16[16,256,128]{2,1,0:T(8,128)(2,1)}), bf16[16,256,128]{2,1,0:T(8,128)(2,1)}, u32[]{:S(2)}, u32[]{:S(2)}) async-start(bf16[16,256,128]{2,1,0:T(8,128)(2,1)} %broadcast_in_dim.46), calls=%async_computation.7 | async-start | bytes 2097152 | tf_op jit(solution)/shard_map/all_to_all | solution.py:24
  63.8 21.9 %collective-permute-start.7 = (bf16[256,1024]{0,1:T(8,128)(2,1)}, bf16[256,1024]{0,1:T(8,128)(2,1)}, u32[]{:S(2)}, u32[]{:S(2)}) collective-permute-start(bf16[256,1024]{0,1:T(8,128)(2,1)} %bitcast.11), channel_id=1, source_target_pairs={{0,1},{1,2},{2,3},{3,4},{4,5},{5,6},{6,7},{7,0},{8,9},{9,10},{10,1... | collective-permute-start | bytes 1572872 | tf_op jit(solution)/shard_map/ppermute | solution.py:88
  66.7 19.0 %collective-permute-start.8 = (bf16[256,1024]{0,1:T(8,128)(2,1)}, bf16[256,1024]{0,1:T(8,128)(2,1)}, u32[]{:S(2)}, u32[]{:S(2)}) collective-permute-start(bf16[256,1024]{0,1:T(8,128)(2,1)} %bitcast.11), channel_id=1, source_target_pairs={{0,7},{1,0},{2,1},{3,2},{4,3},{5,4},{6,5},{7,6},{8,15},{9,8},{10,9... | collective-permute-start | bytes 1572872 | tf_op jit(solution)/shard_map/ppermute | solution.py:95
  70.1 24.0 %collective-permute-start.16 = (bf16[256,1024]{0,1:T(8,128)(2,1)}, bf16[256,1024]{0,1:T(8,128)(2,1)}, u32[]{:S(2)}, u32[]{:S(2)}) collective-permute-start(bf16[256,1024]{0,1:T(8,128)(2,1)} %collective-permute-done.14), channel_id=1, source_target_pairs={{0,1},{1,2},{2,3},{3,4},{4,5},{5,6},{6,7},{7,0},{8,9},{9,10},{10,1... | collective-permute-start | bytes 1572872 | tf_op jit(solution)/shard_map/ppermute | solution.py:88
  74.8 34.9 %collective-permute-start = (bf16[256,2048]{0,1:T(8,128)(2,1)S(1)}, bf16[256,2048]{0,1:T(8,128)(2,1)}, u32[]{:S(2)}, u32[]{:S(2)}) collective-permute-start(bf16[256,2048]{0,1:T(8,128)(2,1)S(1)} %bitcast.84), channel_id=1, source_target_pairs={{0,1},{1,2},{2,3},{3,4},{4,5},{5,6},{6,7},{7,0},{8,9},{9,10},{10,1... | collective-permute-start | bytes 3145736 | tf_op jit(solution)/shard_map/ppermute | solution.py:88
  79.3 18.7 %collective-permute-start.17 = (bf16[256,1024]{0,1:T(8,128)(2,1)}, bf16[256,1024]{0,1:T(8,128)(2,1)}, u32[]{:S(2)}, u32[]{:S(2)}) collective-permute-start(bf16[256,1024]{0,1:T(8,128)(2,1)} %collective-permute-done.15), channel_id=1, source_target_pairs={{0,7},{1,0},{2,1},{3,2},{4,3},{5,4},{6,5},{7,6},{8,15},{9,8},{10,9... | collective-permute-start | bytes 1572872 | tf_op jit(solution)/shard_map/ppermute | solution.py:95
  85.7 26.7 %collective-permute-start.1 = (bf16[256,2048]{0,1:T(8,128)(2,1)S(1)}, bf16[256,2048]{0,1:T(8,128)(2,1)}, u32[]{:S(2)}, u32[]{:S(2)}) collective-permute-start(bf16[256,2048]{0,1:T(8,128)(2,1)S(1)} %bitcast.85), channel_id=1, source_target_pairs={{0,7},{1,0},{2,1},{3,2},{4,3},{5,4},{6,5},{7,6},{8,15},{9,8},{10,9... | collective-permute-start | bytes 3145736 | tf_op jit(solution)/shard_map/ppermute | solution.py:95
  116.3 34.4 %collective-permute-start.2 = (bf16[256,2048]{0,1:T(8,128)(2,1)}, bf16[256,2048]{0,1:T(8,128)(2,1)}, u32[]{:S(2)}, u32[]{:S(2)}) collective-permute-start(bf16[256,2048]{0,1:T(8,128)(2,1)} %collective-permute-done), channel_id=1, source_target_pairs={{0,1},{1,2},{2,3},{3,4},{4,5},{5,6},{6,7},{7,0},{8,9},{9,10},{10,1... | collective-permute-start | bytes 3145736 | tf_op jit(solution)/shard_map/ppermute | solution.py:88
  121.7 22.4 %collective-permute-start.20 = (bf16[256,1024]{0,1:T(8,128)(2,1)S(1)}, bf16[256,1024]{0,1:T(8,128)(2,1)S(1)}, u32[]{:S(2)}, u32[]{:S(2)}) collective-permute-start(bf16[256,1024]{0,1:T(8,128)(2,1)S(1)} %collective-permute-done.18), channel_id=1, source_target_pairs={{0,1},{1,2},{2,3},{3,4},{4,5},{5,6},{6,7},{7,0},{8,9},{9,10},{10,1... | collective-permute-start | bytes 1572872 | tf_op jit(solution)/shard_map/ppermute | solution.py:88
  121.7 28.0 %collective-permute-start.13 = (bf16[256,1024]{0,1:T(8,128)(2,1)S(1)}, bf16[256,1024]{0,1:T(8,128)(2,1)S(1)}, u32[]{:S(2)}, u32[]{:S(2)}) collective-permute-start(bf16[256,1024]{0,1:T(8,128)(2,1)S(1)} %collective-permute-done.11), channel_id=1, source_target_pairs={{0,1},{1,2},{2,3},{3,4},{4,5},{5,6},{6,7},{7,0},{8,9},{9,10},{10,1... | collective-permute-start | bytes 1572872 | tf_op jit(solution)/shard_map/ppermute | solution.py:88
  127.6 43.0 %collective-permute-start.3 = (bf16[256,2048]{0,1:T(8,128)(2,1)}, bf16[256,2048]{0,1:T(8,128)(2,1)}, u32[]{:S(2)}, u32[]{:S(2)}) collective-permute-start(bf16[256,2048]{0,1:T(8,128)(2,1)} %collective-permute-done.1), channel_id=1, source_target_pairs={{0,7},{1,0},{2,1},{3,2},{4,3},{5,4},{6,5},{7,6},{8,15},{9,8},{10,9... | collective-permute-start | bytes 3145736 | tf_op jit(solution)/shard_map/ppermute | solution.py:95
  131.0 51.9 %collective-permute-start.23 = (bf16[256,2048]{0,1:T(8,128)(2,1)}, bf16[256,2048]{0,1:T(8,128)(2,1)}, u32[]{:S(2)}, u32[]{:S(2)}) collective-permute-start(bf16[256,2048]{0,1:T(8,128)(2,1)} %collective-permute-done.21), channel_id=1, source_target_pairs={{0,1},{1,2},{2,3},{3,4},{4,5},{5,6},{6,7},{7,0},{8,9},{9,10},{10,1... | collective-permute-start | bytes 3145736 | tf_op jit(solution)/shard_map/ppermute | solution.py:88
  144.1 99.3 %collective-permute-start.24 = (bf16[256,2048]{0,1:T(8,128)(2,1)}, bf16[256,2048]{0,1:T(8,128)(2,1)}, u32[]{:S(2)}, u32[]{:S(2)}) collective-permute-start(bf16[256,2048]{0,1:T(8,128)(2,1)} %collective-permute-done.22), channel_id=1, source_target_pairs={{0,7},{1,0},{2,1},{3,2},{4,3},{5,4},{6,5},{7,6},{8,15},{9,8},{10,9... | collective-permute-start | bytes 3145736 | tf_op jit(solution)/shard_map/ppermute | solution.py:95
  150.8 21.5 %collective-permute-start.4 = (bf16[256,2048]{0,1:T(8,128)(2,1)}, bf16[256,2048]{0,1:T(8,128)(2,1)}, u32[]{:S(2)}, u32[]{:S(2)}) collective-permute-start(bf16[256,2048]{0,1:T(8,128)(2,1)} %collective-permute-done.2), channel_id=1, source_target_pairs={{0,1},{1,2},{2,3},{3,4},{4,5},{5,6},{6,7},{7,0},{8,9},{9,10},{10,1... | collective-permute-start | bytes 3145736 | tf_op jit(solution)/shard_map/ppermute | solution.py:88
  163.8 41.5 %all-to-all-start.3 = ((bf16[256,16,128]{2,0,1:T(8,128)(2,1)}), bf16[256,16,128]{2,0,1:T(8,128)(2,1)S(1)}, u32[]{:S(2)}, u32[]{:S(2)}) async-start(bf16[256,16,128]{2,0,1:T(8,128)(2,1)} %bitcast.88), calls=%async_computation.3 | async-start | bytes 2097152 | tf_op jit(solution)/shard_map/all_to_all | solution.py:135
  170.6 19.4 %collective-permute-start.5 = (bf16[256,2048]{0,1:T(8,128)(2,1)}, bf16[256,2048]{0,1:T(8,128)(2,1)}, u32[]{:S(2)}, u32[]{:S(2)}) collective-permute-start(bf16[256,2048]{0,1:T(8,128)(2,1)} %collective-permute-done.3), channel_id=1, source_target_pairs={{0,7},{1,0},{2,1},{3,2},{4,3},{5,4},{6,5},{7,6},{8,15},{9,8},{10,9... | collective-permute-start | bytes 3145736 | tf_op jit(solution)/shard_map/ppermute | solution.py:95
  172.2 20.1 %collective-permute-start.6 = (bf16[256,2048]{0,1:T(8,128)(2,1)}, bf16[256,2048]{0,1:T(8,128)(2,1)}, u32[]{:S(2)}, u32[]{:S(2)}) collective-permute-start(bf16[256,2048]{0,1:T(8,128)(2,1)} %collective-permute-done.4), channel_id=1, source_target_pairs={{0,1},{1,2},{2,3},{3,4},{4,5},{5,6},{6,7},{7,0},{8,9},{9,10},{10,1... | collective-permute-start | bytes 3145736 | tf_op jit(solution)/shard_map/ppermute | solution.py:88
  182.9 66.7 %collective-permute-start.25 = (bf16[256,2048]{0,1:T(8,128)(2,1)}, bf16[256,2048]{0,1:T(8,128)(2,1)}, u32[]{:S(2)}, u32[]{:S(2)}) collective-permute-start(bf16[256,2048]{0,1:T(8,128)(2,1)} %collective-permute-done.23), channel_id=1, source_target_pairs={{0,1},{1,2},{2,3},{3,4},{4,5},{5,6},{6,7},{7,0},{8,9},{9,10},{10,1... | collective-permute-start | bytes 3145736 | tf_op jit(solution)/shard_map/ppermute | solution.py:88
  205.3 23.2 %all-to-all-start.5 = ((bf16[256,16,128]{0,2,1:T(8,128)(2,1)}), bf16[256,16,128]{0,2,1:T(8,128)(2,1)}, u32[]{:S(2)}, u32[]{:S(2)}) async-start(bf16[256,16,128]{0,2,1:T(8,128)(2,1)} %bitcast.87), calls=%async_computation.5 | async-start | bytes 2097152 | tf_op jit(solution)/shard_map/all_to_all | solution.py:136
  228.5 22.5 %all-to-all-start.1 = ((bf16[256,16,128]{2,0,1:T(8,128)(2,1)}), bf16[256,16,128]{2,0,1:T(8,128)(2,1)S(1)}, u32[]{:S(2)}, u32[]{:S(2)}) async-start(bf16[256,16,128]{2,0,1:T(8,128)(2,1)} %copy.28), calls=%async_computation.1 | async-start | bytes 2097152 | tf_op jit(solution)/shard_map/all_to_all | solution.py:128
  243.3 63.4 %collective-permute-start.26 = (bf16[256,2048]{0,1:T(8,128)(2,1)}, bf16[256,2048]{0,1:T(8,128)(2,1)}, u32[]{:S(2)}, u32[]{:S(2)}) collective-permute-start(bf16[256,2048]{0,1:T(8,128)(2,1)} %collective-permute-done.24), channel_id=1, source_target_pairs={{0,7},{1,0},{2,1},{3,2},{4,3},{5,4},{6,5},{7,6},{8,15},{9,8},{10,9... | collective-permute-start | bytes 3145736 | tf_op jit(solution)/shard_map/ppermute | solution.py:95
  249.6 59.5 %collective-permute-start.27 = (bf16[256,2048]{0,1:T(8,128)(2,1)}, bf16[256,2048]{0,1:T(8,128)(2,1)}, u32[]{:S(2)}, u32[]{:S(2)}) collective-permute-start(bf16[256,2048]{0,1:T(8,128)(2,1)} %collective-permute-done.25), channel_id=1, source_target_pairs={{0,1},{1,2},{2,3},{3,4},{4,5},{5,6},{6,7},{7,0},{8,9},{9,10},{10,1... | collective-permute-start | bytes 3145736 | tf_op jit(solution)/shard_map/ppermute | solution.py:88
  295.4 26.7 %all-to-all-start.6 = ((bf16[16,256,128]{2,1,0:T(8,128)(2,1)}), bf16[16,256,128]{2,1,0:T(8,128)(2,1)S(1)}, u32[]{:S(2)}, u32[]{:S(2)}) async-start(bf16[16,256,128]{2,1,0:T(8,128)(2,1)} %bitcast.93), calls=%async_computation.6 | async-start | bytes 2097152 | tf_op jit(solution)/shard_map/all_to_all | solution.py:138
  (24 other events, 482.6 us)
